TPU v7x, 32 devices: a whole 2x2x4 slice. The times are simulated.
32 devices in a mesh: sp: 8 (over z, x), tp: 4 (over y, core).
Axes of the slice: x: 2, y: 2, z: 4, core: 2. Of those that a mesh axis runs over, the one named last changes fastest.
Arguments:
- target: bfloat16 [1024, 4096], P('sp', 'tp'), may hold values from -300 to 300
- gain: float32 [4096], P('tp'), may hold values from 0.1 to 1.9
- w_query: bfloat16 [4096, 4096], P('tp'), may hold values from -0.09375 to 0.09375
- queries: bfloat16 [1024, 4096], P('sp', 'tp'), may hold values from -13 to 13
- keys: bfloat16 [4096, 1024], P('sp'), may hold values from -4 to 4
- values: bfloat16 [4096, 1024], P('sp'), may hold values from -4 to 4
- attn_out: bfloat16 [1024, 4096], P('sp', 'tp'), may hold values from -4 to 4
- grad_out: bfloat16 [1024, 4096], P('sp', 'tp'), may hold values from -64 to 64
Outputs:
- grad_rows: bfloat16 [1024, 4096], P('sp', 'tp')
- grad_weight: float32 [4096, 4096], P(('tp', 'sp'))
- grad_keys: float32 [4096, 1024], P(('sp', 'tp'))
- grad_values: float32 [4096, 1024], P(('sp', 'tp'))
All inputs are finite; a program needn't handle non-finite values.
Results may differ from a plain program's by a relative error of at most 0.018.
Values may be sent and summed in bfloat16 or wider, within the bound.
A program may use at most 64 MiB of HBM per device.

v0:
```python
import math

import jax
import jax.numpy as jnp
from jax import lax
from jax.sharding import PartitionSpec as P

WIDTH = 4096
HEADS = 16
KV_HEADS = 4
HEAD_DIM = 256


norm_eps = 1e-06


def merged(part, axis, combine):
    gathered = jax.tree.map(lambda a: lax.all_gather(a, axis), part)

    def take(source):
        return jax.tree.map(lambda a: lax.dynamic_index_in_dim(a, source, 0, False), gathered)

    return lax.fori_loop(
        1, lax.axis_size(axis), lambda source, state: combine(state, take(source)), take(0)
    )


def join_stats(first_part, second_part):
    row_peak = jnp.maximum(first_part[0], second_part[0])
    summed = first_part[1] * jnp.exp(first_part[0] - row_peak) + second_part[1] * jnp.exp(
        second_part[0] - row_peak
    )
    return (row_peak, summed, first_part[2] + second_part[2])


def local(target, gain, w_query, queries, keys, values, attn_out, grad_out):
    local_heads = queries.shape[1] // HEAD_DIM
    group_size = HEADS // KV_HEADS
    score_scale = HEAD_DIM ** (-0.5)
    own_rows = queries.shape[0]
    src_rows = keys.shape[0]
    kv_index = lax.axis_index("tp") * local_heads // group_size
    key_own = lax.dynamic_slice_in_dim(keys, kv_index * HEAD_DIM, HEAD_DIM, 1)
    value_own = lax.dynamic_slice_in_dim(values, kv_index * HEAD_DIM, HEAD_DIM, 1)
    out_heads = attn_out.reshape(own_rows, local_heads, HEAD_DIM).astype(jnp.float32)
    grad_heads = grad_out.reshape(own_rows, local_heads, HEAD_DIM).astype(jnp.float32)
    delta_own = jnp.sum(out_heads * grad_heads, axis=2)
    empty_sum = jnp.zeros((src_rows, HEAD_DIM), jnp.float32)
    total_rows = own_rows * lax.axis_size("sp")
    position = lax.axis_index("sp") * own_rows
    delta_full = lax.dynamic_update_slice_in_dim(
        jnp.zeros((total_rows, local_heads), jnp.float32), delta_own, position, 0
    )
    query_all, grad_all = (
        lax.all_gather(queries, "sp", axis=0, tiled=True),
        lax.all_gather(grad_out, "sp", axis=0, tiled=True),
    )
    block_rows = math.gcd(total_rows, 512)
    block_count = total_rows // block_rows
    query_blocks = query_all.reshape(block_count, block_rows, local_heads, HEAD_DIM)
    grad_blocks = grad_all.reshape(block_count, block_rows, local_heads, HEAD_DIM)

    def block_stats(query_block):
        scores = (
            jnp.einsum("qhd,sd->hqs", query_block, key_own, preferred_element_type=jnp.float32)
            * score_scale
        )
        row_peak = jnp.max(scores, axis=2)
        row_total = jnp.sum(jnp.exp(scores - row_peak[:, :, None]), axis=2)
        return (row_peak, row_total)

    peaks, totals = lax.map(block_stats, query_blocks)
    peaks, totals, delta_full = merged((peaks, totals, delta_full), "sp", join_stats)
    log_totals = peaks + jnp.log(totals)
    delta_blocks = delta_full.reshape(block_count, block_rows, local_heads)

    def block_grads(running, inputs):
        query_block, grad_block, delta_block, log_block = inputs
        scores = (
            jnp.einsum("qhd,sd->hqs", query_block, key_own, preferred_element_type=jnp.float32)
            * score_scale
        )
        weights = jnp.exp(scores - log_block[:, :, None])
        grad_weights = jnp.einsum(
            "qhd,sd->hqs", grad_block, value_own, preferred_element_type=jnp.float32
        )
        delta_cols = jnp.transpose(delta_block)
        grad_scores = (weights * (grad_weights - delta_cols[:, :, None]) * score_scale).astype(
            jnp.bfloat16
        )
        key_sum = running[0] + jnp.einsum(
            "hqs,qhd->sd", grad_scores, query_block, preferred_element_type=jnp.float32
        )
        value_sum = running[1] + jnp.einsum(
            "hqs,qhd->sd",
            weights.astype(jnp.bfloat16),
            grad_block,
            preferred_element_type=jnp.float32,
        )
        query_part = jnp.einsum(
            "hqs,sd->qhd", grad_scores, key_own, preferred_element_type=jnp.float32
        )
        return ((key_sum, value_sum), query_part)

    (key_sum, value_sum), query_parts = lax.scan(
        block_grads, (empty_sum, empty_sum), (query_blocks, grad_blocks, delta_blocks, log_totals)
    )
    query_parts = query_parts.reshape(total_rows, 1, local_heads * HEAD_DIM)
    received = lax.all_to_all(
        query_parts.astype(jnp.bfloat16), "sp", split_axis=0, concat_axis=1, tiled=True
    ).astype(query_parts.dtype)
    query_grad = jnp.sum(received, axis=1)
    key_cols = key_sum.reshape(src_rows, 1, HEAD_DIM)
    value_cols = value_sum.reshape(src_rows, 1, HEAD_DIM)
    key_parts, value_parts = (
        lax.all_to_all(
            key_cols.astype(jnp.bfloat16), "tp", split_axis=0, concat_axis=1, tiled=True
        ).astype(key_cols.dtype),
        lax.all_to_all(
            value_cols.astype(jnp.bfloat16), "tp", split_axis=0, concat_axis=1, tiled=True
        ).astype(value_cols.dtype),
    )
    part_rows = key_parts.shape[0]
    per_kv = key_parts.shape[1] // KV_HEADS
    grad_keys = (
        key_parts.reshape(part_rows, KV_HEADS, per_kv, HEAD_DIM)
        .sum(axis=2)
        .reshape(part_rows, KV_HEADS * HEAD_DIM)
    )
    grad_values = (
        value_parts.reshape(part_rows, KV_HEADS, per_kv, HEAD_DIM)
        .sum(axis=2)
        .reshape(part_rows, KV_HEADS * HEAD_DIM)
    )
    query_grad = query_grad.astype(jnp.bfloat16)
    query_all_heads = lax.all_gather(query_grad, "tp", axis=1, tiled=True)
    grad_rows = lax.dot_general(
        query_all_heads, w_query, (((1,), (1,)), ((), ())), preferred_element_type=jnp.float32
    ).astype(jnp.bfloat16)
    target_wide = target.astype(jnp.float32)
    squares = lax.psum(jnp.sum(target_wide * target_wide, axis=1), "tp")
    inverse = lax.rsqrt(squares / WIDTH + norm_eps)
    normed = (target_wide * inverse[:, None] * gain).astype(jnp.bfloat16)
    grad_weight = lax.psum_scatter(
        lax.dot_general(
            normed, query_all_heads, (((0,), (0,)), ((), ())), preferred_element_type=jnp.float32
        ).astype(jnp.bfloat16),
        "sp",
        scatter_dimension=0,
        tiled=True,
    ).astype(jnp.float32)
    return (grad_rows, grad_weight, grad_keys, grad_values)


def solution(mesh):
    return jax.shard_map(
        local,
        mesh=mesh,
        in_specs=(
            P("sp", "tp"),
            P("tp"),
            P("tp", None),
            P("sp", "tp"),
            P("sp", None),
            P("sp", None),
            P("sp", "tp"),
            P("sp", "tp"),
        ),
        out_specs=(
            P("sp", "tp"),
            P(("tp", "sp"), None),
            P(("sp", "tp"), None),
            P(("sp", "tp"), None),
        ),
        check_vma=False,
    )
```

profile of v0, /device:TPU:24, one launch (start us, length us, event | category | flops | bytes accessed | tf_op | source)
XLA Modules:
  0.0 417.8 jit_solution(14617625495296849069)
XLA Ops:
  10.4 28.0 %all_gather.33 = f32[8,1024,4]{1,2,0:T(4,128)S(1)} all-gather(f32[1,1024,4]{1,2,0:T(4,128)S(1)} %constant_dynamic-update-slice_fusion), channel_id=1, replica_groups=mesh['sp'=8,'tp'=4] {'sp'}, dimensions={0}, use_global_device_ids=true | all-gather | bytes 147456 | tf_op jit(solution)/shard_map/all_gather | solution.py:18
  39.1 1.8 constant_dynamic-slice_fusion.1
  40.9 18.3 %all-gather.6.cloned.1.call-done = bf16[1024,1024]{1,0:T(8,128)(2,1)} async-done(((bf16[128,1024]{1,0:T(8,128)(2,1)}), bf16[1024,1024]{1,0:T(8,128)(2,1)}) %all-gather.6.cloned.1.call-update) | async-done | bytes 2097168 | tf_op jit(solution)/shard_map/all_gather | solution.py:55
  59.1 4.5 %reshape.71 = bf16[2,512,4,256]{3,2,1,0:T(4,128)(2,1)} reshape(bf16[1024,1024]{1,0:T(8,128)(2,1)} %all-gather.6.cloned.1.call-done) | data formatting | bytes 4194304 | tf_op jit(solution)/shard_map/reshape | solution.py:60
  63.6 1.9 copy.38
  65.5 3.0 while.46
  68.5 30.0 %all-gather.1 = f32[16,4,512]{2,1,0:T(4,128)S(1)} all-gather(f32[2,4,512]{2,1,0:T(4,128)S(1)} %get-tuple-element.265), channel_id=3, replica_groups=mesh['sp'=8,'tp'=4] {'sp'}, dimensions={0}, use_global_device_ids=true | all-gather | bytes 147456 | tf_op jit(solution)/shard_map/all_gather | solution.py:18
  98.5 30.8 %all-gather = f32[16,4,512]{2,1,0:T(4,128)S(1)} all-gather(f32[2,4,512]{2,1,0:T(4,128)S(1)} %get-tuple-element.264), channel_id=2, replica_groups=mesh['sp'=8,'tp'=4] {'sp'}, dimensions={0}, use_global_device_ids=true | all-gather | bytes 147456 | tf_op jit(solution)/shard_map/all_gather | solution.py:18
  130.0 10.6 %while.47 = (s32[]{:T(128)}, f32[2,4,512]{2,1,0:T(4,128)S(1)}, f32[2,4,512]{2,1,0:T(4,128)S(1)}, f32[1024,4]{0,1:T(4,128)S(1)}, f32[8,2,4,512]{3,2,1,0:T(4,128)}...) while((s32[]{:T(128)}, f32[2,4,512]{2,1,0:T(4,128)S(1)}, ...), condition=%wide.region_6.7_spmd, body=%wide.region_5.6_spmd.sunk | while | flops 28677 | bytes 147599 | solution.py:23
  140.6 4.5 %reshape.72 = bf16[2,512,4,256]{3,2,1,0:T(4,128)(2,1)} reshape(bf16[1024,1024]{1,0:T(8,128)(2,1)} %all-gather.8.cloned.1.call-done) | data formatting | bytes 4194304 | tf_op jit(solution)/shard_map/reshape | solution.py:61
  145.1 18.0 %while.48 = (s32[]{:T(128)}, f32[512,256]{1,0:T(8,128)S(1)}, f32[512,256]{1,0:T(8,128)S(1)}, bf16[2,512,4,256]{3,1,2,0:T(8,128)(2,1)}, bf16[2,512,4,256]{3,1,2,0...) while((s32[]{:T(128)}, f32[512,256]{1,0:T(8,128)S(1)}, ...), condition=%wide.region_8.9_spmd.clone, body=%wide.region_7.8_spmd.clone.sunk | while | flops 2694316032 | bytes 48029940 | solution.py:105
  145.1 1.6 constant_dynamic-slice_fusion.4
  149.0 1.5 fusion.72
  154.1 1.6 constant_dynamic-slice_fusion.4
  158.0 1.5 fusion.72
  163.1 3.2 copy.40
  166.4 6.3 %convert_element_type.92 = bf16[1024,1,1024]{2,1,0:T(2,128)(2,1)} reshape(bf16[2,512,4,256]{3,2,1,0:T(4,128)(2,1)S(1)} %copy.40) | data formatting | bytes 4194304 | tf_op jit(solution)/shard_map/convert_element_type | solution.py:110
  173.2 12.8 %reduce.4 = bf16[1024,1024]{1,0:T(8,128)(2,1)S(1)} reduce(bf16[1024,1,1024]{2,1,0:T(2,128)(2,1)} %convert_element_type.92, bf16[]{:T(256)} %broadcast.49), dimensions={1}, to_apply=%convert_element_type.92.reduce_sub_computation | reduce | bytes 4194306 | tf_op jit(solution)/shard_map/convert_element_type | solution.py:110
  185.9 3.8 reshape.99
  189.7 39.4 %all_to_all.30 = bf16[8,2,65536]{2,1,0:T(2,128)(2,1)S(1)} all-to-all(bf16[8,2,65536]{2,1,0:T(2,128)(2,1)} %reshape.99), channel_id=1, replica_groups=mesh['sp'=8,'tp'=4] {'sp'}, dimensions={0} | all-to-all | bytes 4194304 | tf_op jit(solution)/shard_map/all_to_all | solution.py:109
  229.1 4.3 %reshape.100 = bf16[1024,1,1024]{2,1,0:T(2,128)(2,1)} reshape(bf16[8,2,65536]{2,1,0:T(2,128)(2,1)S(1)} %all_to_all.30) | data formatting | bytes 4194304
  233.5 3.0 copy.49
  237.8 5.9 %psum.7 = f32[128]{0:T(128)S(1)} all-reduce(f32[128]{0:T(128)S(1)} %fusion.36), channel_id=1, replica_groups=mesh['sp'=8,'tp'=4] {'tp'}, use_global_device_ids=true, to_apply=%region_11.12 | all-reduce | flops 128 | bytes 1024 | tf_op jit(solution)/shard_map/psum | solution.py:141
  243.7 11.9 %all-gather.10.cloned.1.call-done = bf16[128,4096]{1,0:T(8,128)(2,1)} async-done(((bf16[128,1024]{1,0:T(8,128)(2,1)}), bf16[128,4096]{1,0:T(8,128)(2,1)}) %all-gather.10.cloned.1.call-update) | async-done | bytes 1048592 | tf_op jit(solution)/shard_map/all_gather | solution.py:136
  255.6 6.9 %convolution_convert_fusion = bf16[1024,4096]{1,0:T(8,128)(2,1)} fusion(bf16[128,4096]{1,0:T(8,128)(2,1)} %all-gather.10.cloned.1.call-done, bf16[128,1024]{1,0:T(8,128)(2,1)S(1)} %copy-done.3, f32[1024]{0:T(1024)S(1)} %copy-done.8, f32[128]{0:T(128)S(1)} %add_rsqrt_fusion), kind=kOutput, calls=%fused_computation.47 | convolution fusion | flops 1078460416 | bytes 9703936 | tf_op jit(solution)/shard_map/dot_general | solution.py:145
  264.2 3.4 all-to-all-start.1
  269.2 4.3 %all-to-all-done.1 = bf16[4,2,16384]{2,1,0:T(2,128)(2,1)S(1)} async-done(((bf16[4,2,16384]{2,1,0:T(2,128)(2,1)}), bf16[4,2,16384]{2,1,0:T(2,128)(2,1)S(1)}, u32[]{:S(2)}, u32[]{:S(2)}) %all-to-all-start.1) | async-done | bytes 262176 | tf_op jit(solution)/shard_map/all_to_all | solution.py:116
  273.5 3.4 all-to-all-start.2
  279.0 3.9 all-to-all-done.2
  285.0 7.0 %convolution_convert_fusion.1 = bf16[128,1024]{1,0:T(8,128)(2,1)} fusion(bf16[128,4096]{1,0:T(8,128)(2,1)S(1)} %copy-done, bf16[1024,4096]{1,0:T(8,128)(2,1)} %param.16), kind=kOutput, calls=%fused_computation.48 | convolution fusion | flops 1073872896 | bytes 9699328 | tf_op jit(solution)/shard_map/dot_general | solution.py:137
  292.0 116.5 %reduce-scatter.2.cloned.1.call-done = bf16[128,4096]{1,0:T(8,128)(2,1)} async-done(((bf16[1024,4096]{1,0:T(8,128)(2,1)}), bf16[128,4096]{1,0:T(8,128)(2,1)}) %reduce-scatter.2.cloned.1.call-update) | async-done | bytes 1048592 | tf_op jit(solution)/shard_map/reduce_scatter | solution.py:144
  408.5 2.8 convert_element_type.81
  (98 shorter events, 38.7 us)
Async XLA Ops:
  7.2 52.0 %all-gather.6.cloned.1.call-start = ((), (), s32[]{:S(2)}) async-start(), calls=%async_computation.4 | async-start | bytes 2359296 | tf_op jit(solution)/shard_map/all_gather | solution.py:55
  7.9 132.7 %all-gather.8.cloned.1.call-start = ((), (), s32[]{:S(2)}) async-start(), calls=%async_computation.5 | async-start | bytes 2359296 | tf_op jit(solution)/shard_map/all_gather | solution.py:56
  8.6 247.0 %all-gather.10.cloned.1.call-start = ((), (), s32[]{:S(2)}) async-start(), calls=%async_computation.6 | async-start | bytes 1310720 | tf_op jit(solution)/shard_map/all_gather | solution.py:136
  38.4 0.7 copy-start.4
  98.5 30.8 %copy-start.5 = (f32[16,4,512]{2,1,0:T(4,128)}, f32[16,4,512]{2,1,0:T(4,128)S(1)}, u32[]{:S(2)}) copy-start(f32[16,4,512]{2,1,0:T(4,128)S(1)} %all-gather.1) | copy-start | bytes 393220
  129.3 0.7 copy-start.6
  147.5 1.5 copy-start.7
  150.5 1.6 copy-start.1
  152.8 1.3 copy-start.2
  156.5 1.5 copy-start.7
  159.5 1.6 copy-start.1
  161.8 1.3 copy-start.2
  233.5 4.2 %copy-start.3 = (bf16[128,1024]{1,0:T(8,128)(2,1)S(1)}, bf16[128,1024]{1,0:T(8,128)(2,1)}, u32[]{:S(2)}) copy-start(bf16[128,1024]{1,0:T(8,128)(2,1)} %param.14) | copy-start | bytes 786436
  233.5 22.1 %copy-start.8 = (f32[1024]{0:T(1024)S(1)}, f32[1024]{0:T(1024)}, u32[]{:S(2)}) copy-start(f32[1024]{0:T(1024)} %param.15) | copy-start | bytes 12292
  237.6 170.9 %reduce-scatter.2.cloned.1.call-start = ((), (), s32[]{:S(2)}) async-start(), calls=%async_computation.7 | async-start | bytes 9437184 | tf_op jit(solution)/shard_map/reduce_scatter | solution.py:144
  264.2 9.4 %all-to-all-start.1 = ((bf16[4,2,16384]{2,1,0:T(2,128)(2,1)}), bf16[4,2,16384]{2,1,0:T(2,128)(2,1)S(1)}, u32[]{:S(2)}, u32[]{:S(2)}) async-start(bf16[4,2,16384]{2,1,0:T(2,128)(2,1)} %reshape.101), calls=%async_computation.2 | async-start | bytes 524288 | tf_op jit(solution)/shard_map/all_to_all | solution.py:116
  269.2 15.8 %copy-start = (bf16[128,4096]{1,0:T(8,128)(2,1)S(1)}, bf16[128,4096]{1,0:T(8,128)(2,1)}, u32[]{:S(2)}) copy-start(bf16[128,4096]{1,0:T(8,128)(2,1)} %all-gather.10.cloned.1.call-done) | copy-start | bytes 3145732
  273.5 9.4 %all-to-all-start.2 = ((bf16[4,2,16384]{2,1,0:T(2,128)(2,1)}), bf16[4,2,16384]{2,1,0:T(2,128)(2,1)S(1)}, u32[]{:S(2)}, u32[]{:S(2)}) async-start(bf16[4,2,16384]{2,1,0:T(2,128)(2,1)} %reshape.103), calls=%async_computation.3 | async-start | bytes 524288 | tf_op jit(solution)/shard_map/all_to_all | solution.py:119
Sparse Core Ops, SparseCore 0:
  10.1 48.9 all-gather.5
  61.3 49.1 all-gather.7
  237.8 17.7 all-gather.9
  262.7 145.7 reduce-scatter.1
where the time goes:
time: 424 us; the launch traced here: 418 us
  waiting for transfers between devices  156 us (37%)
  blocking collectives  134 us (32%)
  local copies, waits for them, and re-layouts  47.3 us (11%)
  other arithmetic  32.8 us (8%)
  matrix products  26.1 us (6%)
  between operations  14 us (3%)
  starting transfers between devices  6.97 us (2%)
    reduce_scatter x1, waiting for transfers between devices, local(): lax.psum_scatter(lax.dot_general(normed, query_all_heads, (((0,), (0,)),...  116 us
    all_gather x3, blocking collectives, merged(): gathered = jax.tree.map(lambda a: lax.all_gather(a, axis), part)  88.8 us
    all_to_all x1, blocking collectives, local(): lax.all_to_all(query_parts.astype(jnp.bfloat16), 'sp', split_axis=0, conc...  39.4 us
    all_gather x1, waiting for transfers between devices, local(): lax.all_gather(queries, 'sp', axis=0, tiled=True)  18.3 us
    unnamed x22, local copies, waits for them, and re-layouts  18.2 us
    convert_element_type x1, other arithmetic, local(): query_parts.astype(jnp.bfloat16)  12.8 us
    all_gather x1, waiting for transfers between devices, local(): query_all_heads = lax.all_gather(query_grad, 'tp', axis=1, tiled=True)  11.9 us
    convert_element_type x3, local copies, waits for them, and re-layouts, local(): query_parts.astype(jnp.bfloat16)  10 us
  transfers between devices with their start and end apart: 6, of which 5 were waited for; matrix products, arithmetic and copies ran while one was open for 9% of the time, Pallas kernels for 0%

commit v1 on v0

--- a/solution.py
+++ b/solution.py
@@ -1,8 +1,11 @@
+import functools
 import math
 
 import jax
 import jax.numpy as jnp
 from jax import lax
+from jax.experimental import pallas as pl
+from jax.experimental.pallas import tpu as pltpu
 from jax.sharding import PartitionSpec as P
 
 WIDTH = 4096
@@ -152,9 +155,340 @@
     return (grad_rows, grad_weight, grad_keys, grad_values)
 
 
+MESH = pl.DeviceIdType.MESH
+BF16, F32 = jnp.bfloat16, jnp.float32
+NT = (((1,), (1,)), ((), ()))
+X = 2
+CHUNK = 256
+
+
+def fused_kernel(
+    zs, ts, heads,
+    target, gain, w_query, queries, keys, values, attn_out, grad_out,
+    grad_rows, grad_weight, grad_keys, grad_values,
+    qs, dos, outs, kbuf, vbuf, ktr, delta, sbuf, pbuf, dsbuf, qpart, qpart_in,
+    stat, stat_in, ksum, kv_out, kv_in, kv_tp, kv_tp_in, sq, ntr, nall,
+    qg, qt, wbuf, res_out, res_in, send, recv, local_sem,
+):
+    rows = queries.shape[0]
+    src = keys.shape[0]
+    hd = HEAD_DIM
+    width = heads * hd
+    cols = heads * rows
+    part = src // ts
+    feat = target.shape[1] // (zs * X)
+    scale = hd ** (-0.5)
+    sp, tp = lax.axis_index("sp"), lax.axis_index("tp")
+    z, x = sp // X, sp % X
+    counter = [0]
+    pending = []
+
+    def zpeer(d, dx=0):
+        return (((z + d) % zs) * X + (x + dx) % X, tp)
+
+    def tpeer(e):
+        return (sp, (tp + e) % ts)
+
+    def push(source, dest, device):
+        i = counter[0]
+        counter[0] += 1
+        copy = pltpu.make_async_remote_copy(
+            src_ref=source, dst_ref=dest, send_sem=send.at[i], recv_sem=recv.at[i],
+            device_id=device, device_id_type=MESH,
+        )
+        copy.start()
+        pending.append(copy)
+        return copy
+
+    local_count = [0]
+
+    def fetch(source, dest):
+        i = local_count[0]
+        local_count[0] += 1
+        copy = pltpu.make_async_copy(source, dest, local_sem.at[i])
+        copy.start()
+        return copy
+
+    head_col = pl.ds(pl.multiple_of(tp * hd, hd), hd)
+    q_loads, d_loads, o_loads = [], [], []
+    kv_loads = [
+        fetch(keys.at[:, head_col], kbuf.at[pl.ds(0, src)]),
+        fetch(values.at[:, head_col], vbuf.at[pl.ds(0, src)]),
+    ]
+    for ref, buf, loads in ((queries, qs, q_loads), (grad_out, dos, d_loads), (attn_out, outs, o_loads)):
+        for h in range(heads):
+            view = buf.at[pl.ds(h * rows, rows)] if buf is outs else buf.at[0, pl.ds(h * rows, rows)]
+            loads.append(fetch(ref.at[:, pl.ds(h * hd, hd)], view))
+    w_loads = []
+    for e in range(ts):
+        w_col = pl.ds(pl.multiple_of(((tp + ts - e) % ts) * width, width), width)
+        w_loads.append(fetch(w_query.at[:, w_col], wbuf.at[e]))
+
+    barrier = pltpu.get_barrier_semaphore()
+    peers = [zpeer(d, dx) for d in range(zs) for dx in range(X) if d + dx]
+    peers += [tpeer(e) for e in range(1, ts)]
+    for peer in peers:
+        pl.semaphore_signal(barrier, inc=1, device_id=peer, device_id_type=MESH)
+    pl.semaphore_wait(barrier, len(peers))
+
+    order = [1, zs - 1] + list(range(2, zs - 1)) if zs > 2 else list(range(1, zs))
+    for copy in q_loads:
+        copy.wait()
+    q_in = {d: push(qs.at[0], qs.at[d], zpeer(d)) for d in order}
+    for copy in kv_loads:
+        copy.wait()
+    k_in = push(kbuf.at[pl.ds(0, src)], kbuf.at[pl.ds(src, src)], zpeer(0, 1))
+    v_in = push(vbuf.at[pl.ds(0, src)], vbuf.at[pl.ds(src, src)], zpeer(0, 1))
+    for copy in d_loads:
+        copy.wait()
+    do_in = {d: push(dos.at[0], dos.at[d], zpeer(d)) for d in order}
+
+    wide = target[...].astype(F32)
+    sq[0] = jnp.broadcast_to(jnp.sum(wide * wide, axis=1, keepdims=True), (rows, 128))
+    sq_in = [push(sq.at[0], sq.at[e], tpeer(e)) for e in range(1, ts)]
+
+    for copy in o_loads:
+        copy.wait()
+    for h in range(heads):
+        span = pl.ds(h * rows, rows)
+        dot = jnp.sum(dos[0, span].astype(F32) * outs[span].astype(F32), axis=1, keepdims=True)
+        delta[0, :, span] = jnp.broadcast_to(dot, (rows, 128)).T[:8]
+    delta_in = {d: push(delta.at[0], delta.at[d], zpeer(d)) for d in order}
+
+    for copy in sq_in:
+        copy.wait_recv()
+    total = sq[0]
+    for e in range(1, ts):
+        total = total + sq[e]
+    inverse = lax.rsqrt(total[:, :1] / (target.shape[1] * ts) + norm_eps)
+    normed = target[...].astype(F32) * inverse * gain[...]
+    ntr[...] = normed.T.astype(BF16)
+
+    def feature_rows(d, dx):
+        owner = ((z + d) % zs) * X + (x + dx) % X
+        return pl.ds(pl.multiple_of(owner * feat, feat), feat)
+
+    n_in = []
+    for d in range(zs):
+        for dx in range(X):
+            lanes = pl.ds((d * X + dx) * rows, rows)
+            if d + dx:
+                n_in.append(
+                    push(ntr.at[feature_rows(d, dx)], nall.at[0, :, lanes], zpeer(d, dx))
+                )
+            else:
+                nall[0, :, lanes] = ntr[feature_rows(0, 0)]
+
+    ktr[:, :src] = kbuf[:src].T
+    k_in.wait_recv()
+    ktr[:, src:] = kbuf[src:].T
+    v_in.wait_recv()
+    chunks = X * src // CHUNK
+
+    def scores_of(d):
+        def step(c, peak):
+            span = pl.ds(pl.multiple_of(c * CHUNK, CHUNK), CHUNK)
+            s = lax.dot_general(kbuf[span], qs[d], NT, preferred_element_type=F32)
+            sbuf[span] = s
+            return jnp.maximum(peak, jnp.max(s, axis=0, keepdims=True))
+
+        return lax.fori_loop(0, chunks, step, jnp.full((1, cols), -jnp.inf, F32))
+
+    def grads_of(d, peak):
+        own_delta = delta[d, :1]
+
+        def step(c, total):
+            span = pl.ds(pl.multiple_of(c * CHUNK, CHUNK), CHUNK)
+            p = jnp.exp((sbuf[span] - peak) * scale)
+            dp = lax.dot_general(vbuf[span], dos[d], NT, preferred_element_type=F32)
+            pbuf[d, span] = p.astype(BF16)
+            dsbuf[d, span] = (p * (dp - own_delta) * scale).astype(BF16)
+            return total + jnp.sum(p, axis=0, keepdims=True)
+
+        total = lax.fori_loop(0, chunks, step, jnp.zeros((1, cols), F32))
+        stat[d, 0:1] = peak * scale
+        stat[d, 1:2] = total
+        stat[d, 2:8] = jnp.zeros((6, cols), F32)
+        return jnp.dot(ktr[...], dsbuf[d], preferred_element_type=F32)
+
+    qp_in, own_part = {}, None
+    for d in [0] + order:
+        if d:
+            q_in[d].wait_recv()
+        peak = scores_of(d)
+        if d:
+            do_in[d].wait_recv()
+            delta_in[d].wait_recv()
+        part_t = grads_of(d, peak)
+        qpart[d] = part_t.astype(BF16)
+        if d:
+            qp_in[d] = push(qpart.at[d], qpart_in.at[d], zpeer(zs - d))
+        if d == 0:
+            for copy in n_in:
+                copy.wait_recv()
+            nt_in = [push(nall.at[0], nall.at[e], tpeer(e)) for e in range(1, ts)]
+
+    stat_copies = [push(stat, stat_in.at[d], zpeer(d)) for d in order]
+    for copy in stat_copies:
+        copy.wait_recv()
+
+    def stats_of(d, e):
+        ref = stat.at[d] if e == 0 else stat_in.at[e, (d + zs - e) % zs]
+        return ref[0:1], ref[1:2]
+
+    def ratios(d):
+        parts = [stats_of(d, e) for e in range(zs)]
+        top = parts[0][0]
+        for m, _ in parts[1:]:
+            top = jnp.maximum(top, m)
+        factors = [jnp.exp(m - top) for m, _ in parts]
+        summed = sum(f * l for f, (_, l) in zip(factors, parts))
+        return [f / summed for f in factors]
+
+    own_ratios = ratios(0)
+    for d in range(zs):
+        r = own_ratios[0] if d == 0 else ratios(d)[0]
+        r = jnp.broadcast_to(r, (128, cols)).T
+        r = jnp.concatenate([r] * (hd // 128), axis=1)
+        sbuf_q = (qs[d].astype(F32) * r).astype(BF16)
+        sbuf_d = (dos[d].astype(F32) * r).astype(BF16)
+        for i, (left, right) in enumerate(((dsbuf, sbuf_q), (pbuf, sbuf_d))):
+            piece = jnp.dot(left[d], right, preferred_element_type=F32)
+            ksum[i] = piece if d == 0 else ksum[i] + piece
+    kv_out[...] = ksum[:, src:].astype(BF16)
+    kvx_in = push(kv_out, kv_in, zpeer(0, 1))
+
+    grad_t = qpart[0].astype(F32) * own_ratios[0]
+    for d in order:
+        qp_in[d].wait_recv()
+        grad_t = grad_t + qpart_in[d].astype(F32) * own_ratios[(zs - d) % zs]
+    grad_own = grad_t.T
+    for h in range(heads):
+        qg[pl.ds(0, rows), pl.ds(h * hd, hd)] = grad_own[h * rows : (h + 1) * rows].astype(BF16)
+    own = qg.at[pl.ds(0, rows)]
+    slot = lambda d, dx: qg.at[pl.ds((d * X + dx) * rows, rows)]
+    qz_in = {d: push(own, slot(d, 0), zpeer(d)) for d in order}
+    qx_in = {0: push(own, slot(0, 1), zpeer(0, 1))}
+    qt_in = {e: push(own, qt.at[e], tpeer(e)) for e in range(1, ts)}
+
+    kvx_in.wait_recv()
+    for i in range(2):
+        ksum[i, :src] = ksum[i, :src] + kv_in[i].astype(F32)
+    kv_tp[...] = ksum[:, :src].astype(BF16)
+
+    def part_rows(e):
+        return pl.ds(pl.multiple_of(((tp + e) % ts) * part, part), part)
+
+    kvt_in = [push(kv_tp.at[:, part_rows(e)], kv_tp_in.at[e], tpeer(e)) for e in range(1, ts)]
+    for i, out in enumerate((grad_keys, grad_values)):
+        out[:, head_col] = ksum[i, part_rows(0)]
+
+    for d in order[:2]:
+        qz_in[d].wait_recv()
+        qx_in[d] = push(slot(d, 0), slot(d, 1), zpeer(0, 1))
+    w_loads[0].wait()
+    rows_sum = lax.dot_general(own[...], wbuf[0], NT, preferred_element_type=F32)
+    for e in range(1, ts):
+        qt_in[e].wait_recv()
+        w_loads[e].wait()
+        rows_sum = rows_sum + lax.dot_general(qt[e], wbuf[e], NT, preferred_element_type=F32)
+    grad_rows[...] = rows_sum.astype(BF16)
+    for d in order[2:]:
+        qz_in[d].wait_recv()
+        qx_in[d] = push(slot(d, 0), slot(d, 1), zpeer(0, 1))
+    for e in range(1, ts):
+        kvt_in[e - 1].wait_recv()
+        at = pl.ds(pl.multiple_of(((tp + ts - e) % ts) * hd, hd), hd)
+        for i, out in enumerate((grad_keys, grad_values)):
+            out[:, at] = kv_tp_in[e, i].astype(F32)
+    for copy in nt_in:
+        copy.wait_recv()
+    for d in [0] + order:
+        qx_in[d].wait_recv()
+    res_copies = {}
+    for e in [*range(1, ts), 0]:
+        piece = jnp.dot(nall[e], qg[...], preferred_element_type=F32)
+        if e:
+            res_out[e] = piece.astype(BF16)
+            res_copies[e] = push(res_out.at[e], res_in.at[e], tpeer(ts - e))
+        else:
+            grad_weight[:, pl.ds(pl.multiple_of(tp * width, width), width)] = piece
+    for e in range(1, ts):
+        res_copies[e].wait_recv()
+        at = pl.ds(pl.multiple_of(((tp + e) % ts) * width, width), width)
+        grad_weight[:, at] = res_in[e].astype(F32)
+    for copy in pending:
+        copy.wait_send()
+
+
+def fused(target, gain, w_query, queries, keys, values, attn_out, grad_out):
+    zs, ts = lax.axis_size("sp") // X, lax.axis_size("tp")
+    rows, width = queries.shape
+    src = keys.shape[0]
+    heads = width // HEAD_DIM
+    cols, hd = heads * rows, HEAD_DIM
+    feats = target.shape[1]
+    feat = feats // (zs * X)
+    part = src // ts
+    copies = 6 * zs * X + 8 * ts + 16
+    vmem, hbm = pl.BlockSpec(memory_space=pltpu.VMEM), pl.BlockSpec(memory_space=pl.ANY)
+    return pl.pallas_call(
+        functools.partial(fused_kernel, zs, ts, heads),
+        out_shape=(
+            jax.ShapeDtypeStruct((rows, feats), BF16),
+            jax.ShapeDtypeStruct((feat, width * ts), F32),
+            jax.ShapeDtypeStruct((part, keys.shape[1]), F32),
+            jax.ShapeDtypeStruct((part, keys.shape[1]), F32),
+        ),
+        in_specs=[vmem, vmem, hbm, hbm, hbm, hbm, hbm, hbm],
+        out_specs=(vmem,) * 4,
+        scratch_shapes=[
+            pltpu.VMEM((zs, cols, hd), BF16),
+            pltpu.VMEM((zs, cols, hd), BF16),
+            pltpu.VMEM((cols, hd), BF16),
+            pltpu.VMEM((X * src, hd), BF16),
+            pltpu.VMEM((X * src, hd), BF16),
+            pltpu.VMEM((hd, X * src), BF16),
+            pltpu.VMEM((zs, 8, cols), F32),
+            pltpu.VMEM((X * src, cols), F32),
+            pltpu.VMEM((zs, X * src, cols), BF16),
+            pltpu.VMEM((zs, X * src, cols), BF16),
+            pltpu.VMEM((zs, hd, cols), BF16),
+            pltpu.VMEM((zs, hd, cols), BF16),
+            pltpu.VMEM((zs, 8, cols), F32),
+            pltpu.VMEM((zs, zs, 8, cols), F32),
+            pltpu.VMEM((2, X * src, hd), F32),
+            pltpu.VMEM((2, src, hd), BF16),
+            pltpu.VMEM((2, src, hd), BF16),
+            pltpu.VMEM((2, src, hd), BF16),
+            pltpu.VMEM((ts, 2, part, hd), BF16),
+            pltpu.VMEM((ts, rows, 128), F32),
+            pltpu.VMEM((feats, rows), BF16),
+            pltpu.VMEM((ts, feat, zs * X * rows), BF16),
+            pltpu.VMEM((zs * X * rows, width), BF16),
+            pltpu.VMEM((ts, rows, width), BF16),
+            pltpu.VMEM((ts, feats, width), BF16),
+            pltpu.VMEM((ts, feat, width), BF16),
+            pltpu.VMEM((ts, feat, width), BF16),
+            pltpu.SemaphoreType.DMA((copies,)),
+            pltpu.SemaphoreType.DMA((copies,)),
+            pltpu.SemaphoreType.DMA((2 + 3 * heads + ts,)),
+        ],
+        compiler_params=pltpu.CompilerParams(
+            collective_id=0, has_side_effects=True, vmem_limit_bytes=60 * 2**20
+        ),
+    )(target, gain.reshape(1, feats), w_query, queries, keys, values, attn_out, grad_out)
+
+
+def fits(mesh):
+    sp, tp = mesh.shape["sp"], mesh.shape["tp"]
+    feat = WIDTH // (sp * tp)
+    return tp == KV_HEADS and sp % X == 0 and sp > X and feat % 128 == 0
+
+
 def solution(mesh):
     return jax.shard_map(
-        local,
+        fused if fits(mesh) else local,
         mesh=mesh,
         in_specs=(
             P("sp", "tp"),

time: 424 us -> 153 us (0.36); the launches traced: 418 us -> 152 us
  waiting for transfers between devices: 156 us -> 0 us
  Pallas kernels: 0 us -> 145 us
  blocking collectives: 134 us -> 0 us
  local copies, waits for them, and re-layouts: 47.3 us -> 6.46 us
  other arithmetic: 32.8 us -> 0 us
  matrix products: 26.1 us -> 0 us
  between operations: 14 us -> 0.65 us
  starting transfers between devices: 6.97 us -> 0 us
    pallas_call x0 -> x1, Pallas kernels: none -> 145 us  [fused(): pl.pallas_call(functools.partial(fused_kernel, zs, ts, heads), out_shape=...]
    reduce_scatter x1 -> x0, waiting for transfers between devices: 116 us -> none  [local(): lax.psum_scatter(lax.dot_general(normed, query_all_heads, (((0,), (0,)),...]
    all_gather x3 -> x0, blocking collectives: 88.8 us -> none  [merged(): gathered = jax.tree.map(lambda a: lax.all_gather(a, axis), part)]
    all_to_all x1 -> x0, blocking collectives: 39.4 us -> none  [local(): lax.all_to_all(query_parts.astype(jnp.bfloat16), 'sp', split_axis=0, conc...]
    all_gather x3 -> x0, waiting for transfers between devices: 30.2 us -> none  [the longest x1 18.3 us: local(): lax.all_gather(queries, 'sp', axis=0, tiled=True)]
    dot_general x14 -> x0, matrix products: 26.1 us -> none  [the longest x1 7.04 us: local(): lax.dot_general(query_all_heads, w_query, (((1,), (1,)), ((), ())), prefe...]
    convert_element_type x6 -> x0, other arithmetic: 17.2 us -> none  [the longest x1 12.8 us: local(): query_parts.astype(jnp.bfloat16)]
    unnamed x22 -> x8, local copies, waits for them, and re-layouts: 18.2 us -> 6.46 us
  transfers between devices with their start and end apart: 6 -> 0, of which waited for: 5 -> 0; matrix products, arithmetic and copies ran while one was open for 9% -> 0% of each run, Pallas kernels for 0% -> 0%
where the time goes in v1:
time: 153 us; the launch traced here: 152 us
  Pallas kernels  145 us (95%)
  local copies, waits for them, and re-layouts  6.46 us (4%)
    pallas_call x1, Pallas kernels, fused(): pl.pallas_call(functools.partial(fused_kernel, zs, ts, heads), out_shape=...  145 us
    unnamed x8, local copies, waits for them, and re-layouts  6.46 us

profile of v1, /device:TPU:24, one launch (start us, length us, event | category | flops | bytes accessed | tf_op | source)
XLA Modules:
  0.0 152.4 jit_solution(8536818600056581548)
XLA Ops:
  0.6 145.3 %shard_map.111 = (bf16[128,1024]{1,0:T(8,128)(2,1)}, f32[128,4096]{1,0:T(8,128)}, f32[128,1024]{1,0:T(8,128)}, f32[128,1024]{1,0:T(8,128)}) custom-call(bf16[128,1024]{1,0:T(8,128)(2,1)} %target.1, f32[1,1024]{1,0:T(1,128)} %bitcast.1, bf16[1024,4096]{1,0:T(8,128)(2,1)} %w_query.1, bf16[128,1024]{1,0:T(8,128)(2,1)} %queries.1, bf16[512,1024]{1,0:T(8,128)(2,1)} %keys.1, ...), custom_call_target="tpu_custom_call" | custom-call | tf_op jit(solution)/shard_map/pallas_call | solution.py:435
  145.9 1.7 %copy.16 = bf16[128,1024]{1,0:T(8,128)(2,1)} copy(bf16[128,1024]{1,0:T(8,128)(2,1)} %get-tuple-element.8) | data formatting | bytes 524288
  147.6 0.0 copy-start.1
  147.6 0.0 copy-start
  147.6 3.2 %copy.17 = f32[128,4096]{1,0:T(8,128)} copy(f32[128,4096]{1,0:T(8,128)} %get-tuple-element.9) | data formatting | bytes 4194304
  150.8 0.0 copy-done.1
  150.8 0.8 copy.18
  151.6 0.0 copy-done
  151.6 0.8 copy.19
Async XLA Ops:
  147.6 3.2 %copy-start.1 = (f32[128,1024]{1,0:T(8,128)S(1)}, f32[128,1024]{1,0:T(8,128)}, u32[]{:S(2)}) copy-start(f32[128,1024]{1,0:T(8,128)} %get-tuple-element.10) | copy-start | bytes 1572868
  147.6 4.0 %copy-start = (f32[128,1024]{1,0:T(8,128)S(1)}, f32[128,1024]{1,0:T(8,128)}, u32[]{:S(2)}) copy-start(f32[128,1024]{1,0:T(8,128)} %get-tuple-element.11) | copy-start | bytes 1572868

commit v2 on v1

--- a/solution.py
+++ b/solution.py
@@ -168,7 +168,7 @@
     grad_rows, grad_weight, grad_keys, grad_values,
     qs, dos, outs, kbuf, vbuf, ktr, delta, sbuf, pbuf, dsbuf, qpart, qpart_in,
     stat, stat_in, ksum, kv_out, kv_in, kv_tp, kv_tp_in, sq, ntr, nall,
-    qg, qt, wbuf, res_out, res_in, send, recv, local_sem,
+    qown, qg, qt, wbuf, res_out, res_in, send, recv, local_sem, zsend, zrecv, psend, precv, qxs, qxr,
 ):
     rows = queries.shape[0]
     src = keys.shape[0]
@@ -199,6 +199,50 @@
         copy.start()
         pending.append(copy)
         return copy
+
+    def run(device, source, dest, ssem, rsem):
+        return pltpu.make_async_remote_copy(
+            src_ref=source, dst_ref=dest, send_sem=ssem, recv_sem=rsem,
+            device_id=device, device_id_type=MESH,
+        )
+
+    first = (zs - 1 - z) // (zs - 1)
+    last = z // (zs - 1)
+    inner = first + last == 0
+    near = [1 + 2 * first, 3 - first - last, 2 - first + last]
+
+    def hops(stream, view, d):
+        up = run(
+            zpeer(1), view(d), view((d + 1) % zs), zsend.at[stream, d, 0],
+            zrecv.at[stream, (d + 1) % zs],
+        )
+        down = run(
+            zpeer(zs - 1), view(d), view((d + zs - 1) % zs), zsend.at[stream, d, 1],
+            zrecv.at[stream, (d + zs - 1) % zs],
+        )
+        below, above = z >= d, z < d
+        if isinstance(d, int) and d == 0:
+            above = z >= 0
+        return ((up, below & (z < zs - 1)), (down, above & (z > 0)))
+
+    def forward(stream, view, d):
+        for copy, wanted in hops(stream, view, d):
+            pl.when(wanted)(copy.start)
+
+    def arrived(stream, view, d):
+        run(zpeer(1), view(0), view(d), zsend.at[stream, 0, 0], zrecv.at[stream, d]).wait_recv()
+
+    def relay(stream, view, d):
+        arrived(stream, view, d)
+        forward(stream, view, d)
+
+    q_view, d_view = (lambda d: qs.at[d]), (lambda d: dos.at[d])
+    half = width // 2
+
+    def g_view(b, dx=0):
+        return lambda d: qg.at[b, pl.ds(pl.multiple_of((d * X + dx) * rows, rows), rows)]
+
+    streams = ((0, q_view), (1, d_view), (2, g_view(0)), (3, g_view(1)))
 
     local_count = [0]
 
@@ -234,14 +278,14 @@
     order = [1, zs - 1] + list(range(2, zs - 1)) if zs > 2 else list(range(1, zs))
     for copy in q_loads:
         copy.wait()
-    q_in = {d: push(qs.at[0], qs.at[d], zpeer(d)) for d in order}
+    forward(0, q_view, 0)
     for copy in kv_loads:
         copy.wait()
     k_in = push(kbuf.at[pl.ds(0, src)], kbuf.at[pl.ds(src, src)], zpeer(0, 1))
     v_in = push(vbuf.at[pl.ds(0, src)], vbuf.at[pl.ds(src, src)], zpeer(0, 1))
     for copy in d_loads:
         copy.wait()
-    do_in = {d: push(dos.at[0], dos.at[d], zpeer(d)) for d in order}
+    forward(1, d_view, 0)
 
     wide = target[...].astype(F32)
     sq[0] = jnp.broadcast_to(jnp.sum(wide * wide, axis=1, keepdims=True), (rows, 128))
@@ -279,10 +323,6 @@
             else:
                 nall[0, :, lanes] = ntr[feature_rows(0, 0)]
 
-    ktr[:, :src] = kbuf[:src].T
-    k_in.wait_recv()
-    ktr[:, src:] = kbuf[src:].T
-    v_in.wait_recv()
     chunks = X * src // CHUNK
 
     def scores_of(d):
@@ -311,22 +351,58 @@
         stat[d, 2:8] = jnp.zeros((6, cols), F32)
         return jnp.dot(ktr[...], dsbuf[d], preferred_element_type=F32)
 
-    qp_in, own_part = {}, None
-    for d in [0] + order:
-        if d:
-            q_in[d].wait_recv()
+    def process(d):
         peak = scores_of(d)
-        if d:
-            do_in[d].wait_recv()
-            delta_in[d].wait_recv()
-        part_t = grads_of(d, peak)
-        qpart[d] = part_t.astype(BF16)
-        if d:
-            qp_in[d] = push(qpart.at[d], qpart_in.at[d], zpeer(zs - d))
-        if d == 0:
-            for copy in n_in:
-                copy.wait_recv()
-            nt_in = [push(nall.at[0], nall.at[e], tpeer(e)) for e in range(1, ts)]
+        qpart[d] = grads_of(d, peak).astype(BF16)
+
+    def part_copy(d):
+        return run(zpeer(zs - d), qpart.at[d], qpart_in.at[d], psend.at[d], precv.at[d])
+
+    relay(0, q_view, near[0])
+    ktr[:, :src] = kbuf[:src].T
+    k_in.wait_recv()
+    ktr[:, src:] = kbuf[src:].T
+    relay(1, d_view, near[0])
+    v_in.wait_recv()
+
+    @pl.when(inner)
+    def _():
+        relay(0, q_view, near[1])
+        relay(1, d_view, near[1])
+
+    for copy in delta_in.values():
+        copy.wait_recv()
+    process(0)
+
+    @pl.when(inner)
+    def _():
+        relay(0, q_view, near[2])
+
+    process(near[0])
+    part_copy(near[0]).start()
+
+    @pl.when(inner)
+    def _():
+        relay(1, d_view, near[2])
+
+    @pl.when(first + last > 0)
+    def _():
+        arrived(0, q_view, near[1])
+        arrived(1, d_view, near[1])
+
+    process(near[1])
+    part_copy(near[1]).start()
+
+    @pl.when(first + last > 0)
+    def _():
+        arrived(0, q_view, near[2])
+        arrived(1, d_view, near[2])
+
+    process(near[2])
+    part_copy(near[2]).start()
+    for copy in n_in:
+        copy.wait_recv()
+    nt_in = [push(nall.at[0], nall.at[e], tpeer(e)) for e in range(1, ts)]
 
     stat_copies = [push(stat, stat_in.at[d], zpeer(d)) for d in order]
     for copy in stat_copies:
@@ -360,16 +436,24 @@
 
     grad_t = qpart[0].astype(F32) * own_ratios[0]
     for d in order:
-        qp_in[d].wait_recv()
+        part_copy(d).wait_recv()
         grad_t = grad_t + qpart_in[d].astype(F32) * own_ratios[(zs - d) % zs]
     grad_own = grad_t.T
     for h in range(heads):
-        qg[pl.ds(0, rows), pl.ds(h * hd, hd)] = grad_own[h * rows : (h + 1) * rows].astype(BF16)
-    own = qg.at[pl.ds(0, rows)]
-    slot = lambda d, dx: qg.at[pl.ds((d * X + dx) * rows, rows)]
-    qz_in = {d: push(own, slot(d, 0), zpeer(d)) for d in order}
-    qx_in = {0: push(own, slot(0, 1), zpeer(0, 1))}
-    qt_in = {e: push(own, qt.at[e], tpeer(e)) for e in range(1, ts)}
+        piece = grad_own[h * rows : (h + 1) * rows].astype(BF16)
+        qown[:, pl.ds(h * hd, hd)] = piece
+        b, at = h * hd // half, h * hd % half
+        qg[b, pl.ds(0, rows), pl.ds(at, hd)] = piece
+    def cross(b, d):
+        run(zpeer(0, 1), g_view(b)(d), g_view(b, 1)(d), qxs.at[b, d], qxr.at[b, d]).start()
+
+    forward(2, g_view(0), 0)
+    cross(0, 0)
+    qt_in = {e: push(qown, qt.at[e], tpeer(e)) for e in range(1, ts)}
+    relay(2, g_view(0), near[0])
+    forward(3, g_view(1), 0)
+    cross(0, near[0])
+    cross(1, 0)
 
     kvx_in.wait_recv()
     for i in range(2):
@@ -383,19 +467,16 @@
     for i, out in enumerate((grad_keys, grad_values)):
         out[:, head_col] = ksum[i, part_rows(0)]
 
-    for d in order[:2]:
-        qz_in[d].wait_recv()
-        qx_in[d] = push(slot(d, 0), slot(d, 1), zpeer(0, 1))
     w_loads[0].wait()
-    rows_sum = lax.dot_general(own[...], wbuf[0], NT, preferred_element_type=F32)
-    for e in range(1, ts):
-        qt_in[e].wait_recv()
-        w_loads[e].wait()
-        rows_sum = rows_sum + lax.dot_general(qt[e], wbuf[e], NT, preferred_element_type=F32)
-    grad_rows[...] = rows_sum.astype(BF16)
-    for d in order[2:]:
-        qz_in[d].wait_recv()
-        qx_in[d] = push(slot(d, 0), slot(d, 1), zpeer(0, 1))
+    rows_sum = lax.dot_general(qown[...], wbuf[0], NT, preferred_element_type=F32)
+    relay(2, g_view(0), near[1])
+    cross(0, near[1])
+    relay(3, g_view(1), near[0])
+    cross(1, near[0])
+    relay(2, g_view(0), near[2])
+    cross(0, near[2])
+    relay(3, g_view(1), near[1])
+    cross(1, near[1])
     for e in range(1, ts):
         kvt_in[e - 1].wait_recv()
         at = pl.ds(pl.multiple_of(((tp + ts - e) % ts) * hd, hd), hd)
@@ -403,20 +484,46 @@
             out[:, at] = kv_tp_in[e, i].astype(F32)
     for copy in nt_in:
         copy.wait_recv()
-    for d in [0] + order:
-        qx_in[d].wait_recv()
+    def crossed(b):
+        for d in range(zs):
+            run(zpeer(0, 1), g_view(b)(d), g_view(b, 1)(d), qxs.at[b, d], qxr.at[b, d]).wait_recv()
+
     res_copies = {}
-    for e in [*range(1, ts), 0]:
-        piece = jnp.dot(nall[e], qg[...], preferred_element_type=F32)
-        if e:
-            res_out[e] = piece.astype(BF16)
-            res_copies[e] = push(res_out.at[e], res_in.at[e], tpeer(ts - e))
-        else:
-            grad_weight[:, pl.ds(pl.multiple_of(tp * width, width), width)] = piece
+
+    def project(b):
+        for e in [*range(1, ts), 0]:
+            piece = jnp.dot(nall[e], qg[b], preferred_element_type=F32)
+            if e:
+                res_out[b, e] = piece.astype(BF16)
+                res_copies[b, e] = push(res_out.at[b, e], res_in.at[b, e], tpeer(ts - e))
+            else:
+                grad_weight[:, pl.ds(pl.multiple_of(tp * width + b * half, half), half)] = piece
+
+    crossed(0)
+    project(0)
+    relay(3, g_view(1), near[2])
+    cross(1, near[2])
     for e in range(1, ts):
-        res_copies[e].wait_recv()
-        at = pl.ds(pl.multiple_of(((tp + e) % ts) * width, width), width)
-        grad_weight[:, at] = res_in[e].astype(F32)
+        qt_in[e].wait_recv()
+        w_loads[e].wait()
+        rows_sum = rows_sum + lax.dot_general(qt[e], wbuf[e], NT, preferred_element_type=F32)
+    grad_rows[...] = rows_sum.astype(BF16)
+    crossed(1)
+    project(1)
+    for b in range(2):
+        for e in range(1, ts):
+            res_copies[b, e].wait_recv()
+            at = ((tp + e) % ts) * width + b * half
+            grad_weight[:, pl.ds(pl.multiple_of(at, half), half)] = res_in[b, e].astype(F32)
+    for stream, view in streams:
+        for d in range(zs):
+            for copy, wanted in hops(stream, view, d):
+                pl.when(wanted)(copy.wait_send)
+    for d in range(1, zs):
+        part_copy(d).wait_send()
+    for b in range(2):
+        for d in range(zs):
+            run(zpeer(0, 1), g_view(b)(d), g_view(b, 1)(d), qxs.at[b, d], qxr.at[b, d]).wait_send()
     for copy in pending:
         copy.wait_send()
 
@@ -465,14 +572,21 @@
             pltpu.VMEM((ts, rows, 128), F32),
             pltpu.VMEM((feats, rows), BF16),
             pltpu.VMEM((ts, feat, zs * X * rows), BF16),
-            pltpu.VMEM((zs * X * rows, width), BF16),
+            pltpu.VMEM((rows, width), BF16),
+            pltpu.VMEM((2, zs * X * rows, width // 2), BF16),
             pltpu.VMEM((ts, rows, width), BF16),
             pltpu.VMEM((ts, feats, width), BF16),
-            pltpu.VMEM((ts, feat, width), BF16),
-            pltpu.VMEM((ts, feat, width), BF16),
+            pltpu.VMEM((2, ts, feat, width // 2), BF16),
+            pltpu.VMEM((2, ts, feat, width // 2), BF16),
             pltpu.SemaphoreType.DMA((copies,)),
             pltpu.SemaphoreType.DMA((copies,)),
             pltpu.SemaphoreType.DMA((2 + 3 * heads + ts,)),
+            pltpu.SemaphoreType.DMA((4, zs, 2)),
+            pltpu.SemaphoreType.DMA((4, zs)),
+            pltpu.SemaphoreType.DMA((zs,)),
+            pltpu.SemaphoreType.DMA((zs,)),
+            pltpu.SemaphoreType.DMA((2, zs)),
+            pltpu.SemaphoreType.DMA((2, zs)),
         ],
         compiler_params=pltpu.CompilerParams(
             collective_id=0, has_side_effects=True, vmem_limit_bytes=60 * 2**20
@@ -483,7 +597,7 @@
 def fits(mesh):
     sp, tp = mesh.shape["sp"], mesh.shape["tp"]
     feat = WIDTH // (sp * tp)
-    return tp == KV_HEADS and sp % X == 0 and sp > X and feat % 128 == 0
+    return tp == KV_HEADS and sp == 4 * X and feat % 128 == 0
 
 
 def solution(mesh):

time: 153 us -> 136 us (0.89)
  Pallas kernels: 145 us -> 128 us
    pallas_call x1, Pallas kernels: 145 us -> 128 us  [fused(): pl.pallas_call(functools.partial(fused_kernel, zs, ts, heads), out_shape=...]
where the time goes in v2:
time: 136 us; the launch traced here: 135 us
  Pallas kernels  128 us (94%)
  local copies, waits for them, and re-layouts  6.46 us (5%)
    pallas_call x1, Pallas kernels, fused(): pl.pallas_call(functools.partial(fused_kernel, zs, ts, heads), out_shape=...  128 us
    unnamed x8, local copies, waits for them, and re-layouts  6.46 us

profile of v2, /device:TPU:24, one launch (start us, length us, event | category | flops | bytes accessed | tf_op | source)
XLA Modules:
  0.0 135.4 jit_solution(2351432008982683415)
XLA Ops:
  0.6 128.3 %shard_map.111 = (bf16[128,1024]{1,0:T(8,128)(2,1)}, f32[128,4096]{1,0:T(8,128)}, f32[128,1024]{1,0:T(8,128)}, f32[128,1024]{1,0:T(8,128)}) custom-call(bf16[128,1024]{1,0:T(8,128)(2,1)} %target.1, f32[1,1024]{1,0:T(1,128)} %bitcast.1, bf16[1024,4096]{1,0:T(8,128)(2,1)} %w_query.1, bf16[128,1024]{1,0:T(8,128)(2,1)} %queries.1, bf16[512,1024]{1,0:T(8,128)(2,1)} %keys.1, ...), custom_call_target="tpu_custom_call" | custom-call | tf_op jit(solution)/shard_map/pallas_call | solution.py:542
  128.9 1.7 %copy.16 = bf16[128,1024]{1,0:T(8,128)(2,1)} copy(bf16[128,1024]{1,0:T(8,128)(2,1)} %get-tuple-element.8) | data formatting | bytes 524288
  130.6 0.0 copy-start.1
  130.6 0.0 copy-start
  130.6 3.2 %copy.17 = f32[128,4096]{1,0:T(8,128)} copy(f32[128,4096]{1,0:T(8,128)} %get-tuple-element.9) | data formatting | bytes 4194304
  133.8 0.0 copy-done.1
  133.8 0.8 copy.18
  134.6 0.0 copy-done
  134.6 0.8 copy.19
Async XLA Ops:
  130.6 3.2 %copy-start.1 = (f32[128,1024]{1,0:T(8,128)S(1)}, f32[128,1024]{1,0:T(8,128)}, u32[]{:S(2)}) copy-start(f32[128,1024]{1,0:T(8,128)} %get-tuple-element.10) | copy-start | bytes 1572868
  130.6 4.0 %copy-start = (f32[128,1024]{1,0:T(8,128)S(1)}, f32[128,1024]{1,0:T(8,128)}, u32[]{:S(2)}) copy-start(f32[128,1024]{1,0:T(8,128)} %get-tuple-element.11) | copy-start | bytes 1572868

commit v3 on v2

--- a/solution.py
+++ b/solution.py
@@ -528,6 +528,11 @@
         copy.wait_send()
 
 
+def hand_over(*refs):
+    for source, dest in zip(refs[:4], refs[4:]):
+        dest[...] = source[...]
+
+
 def fused(target, gain, w_query, queries, keys, values, attn_out, grad_out):
     zs, ts = lax.axis_size("sp") // X, lax.axis_size("tp")
     rows, width = queries.shape
@@ -539,7 +544,7 @@
     part = src // ts
     copies = 6 * zs * X + 8 * ts + 16
     vmem, hbm = pl.BlockSpec(memory_space=pltpu.VMEM), pl.BlockSpec(memory_space=pl.ANY)
-    return pl.pallas_call(
+    results = pl.pallas_call(
         functools.partial(fused_kernel, zs, ts, heads),
         out_shape=(
             jax.ShapeDtypeStruct((rows, feats), BF16),
@@ -592,6 +597,13 @@
             collective_id=0, has_side_effects=True, vmem_limit_bytes=60 * 2**20
         ),
     )(target, gain.reshape(1, feats), w_query, queries, keys, values, attn_out, grad_out)
+    return pl.pallas_call(
+        hand_over,
+        out_shape=tuple(jax.ShapeDtypeStruct(r.shape, r.dtype) for r in results),
+        in_specs=[vmem] * 4,
+        out_specs=(vmem,) * 4,
+        compiler_params=pltpu.CompilerParams(vmem_limit_bytes=16 * 2**20),
+    )(*results)
 
 
 def fits(mesh):

time: 136 us -> 136 us (level)
  Pallas kernels: 128 us -> 130 us
  local copies, waits for them, and re-layouts: 6.46 us -> 4.62 us
    pallas_call x0 -> x1, Pallas kernels: none -> 1.96 us  [fused(): pl.pallas_call(hand_over, out_shape=tuple((jax.ShapeDtypeStruct(r.shape,...]
    unnamed x8, local copies, waits for them, and re-layouts: 6.46 us -> 4.62 us
where the time goes in v3:
time: 136 us
  Pallas kernels  130 us (96%)
  local copies, waits for them, and re-layouts  4.62 us (3%)
    pallas_call x1, Pallas kernels, fused(): pl.pallas_call(functools.partial(fused_kernel, zs, ts, heads), out_shape=...  128 us
    unnamed x8, local copies, waits for them, and re-layouts  4.62 us

profile of v3, /device:TPU:24, one launch (start us, length us, event | category | flops | bytes accessed | tf_op | source)
XLA Modules:
  0.0 135.5 jit_solution(17209618183073735828)
XLA Ops:
  0.6 128.3 %shard_map.111 = (bf16[128,1024]{1,0:T(8,128)(2,1)}, f32[128,4096]{1,0:T(8,128)}, f32[128,1024]{1,0:T(8,128)}, f32[128,1024]{1,0:T(8,128)}) custom-call(bf16[128,1024]{1,0:T(8,128)(2,1)} %target.1, f32[1,1024]{1,0:T(1,128)} %bitcast.1, bf16[1024,4096]{1,0:T(8,128)(2,1)} %w_query.1, bf16[128,1024]{1,0:T(8,128)(2,1)} %queries.1, bf16[512,1024]{1,0:T(8,128)(2,1)} %keys.1, ...), custom_call_target="tpu_custom_call" | custom-call | tf_op jit(solution)/shard_map/pallas_call | solution.py:547
  128.9 0.0 copy-start
  128.9 1.6 %copy-done = f32[128,4096]{1,0:T(8,128)S(1)} copy-done((f32[128,4096]{1,0:T(8,128)S(1)}, f32[128,4096]{1,0:T(8,128)}, u32[]{:S(2)}) %copy-start) | copy-done | bytes 2097176
  130.5 0.0 copy-start.1
  130.5 1.0 copy-done.1
  131.6 0.0 copy-start.2
  131.6 1.0 copy-done.2
  132.6 0.0 copy-start.3
  132.6 0.9 copy-done.3
  133.6 2.0 %shard_map.112 = (bf16[128,1024]{1,0:T(8,128)(2,1)}, f32[128,4096]{1,0:T(8,128)}, f32[128,1024]{1,0:T(8,128)}, f32[128,1024]{1,0:T(8,128)}) custom-call(bf16[128,1024]{1,0:T(8,128)(2,1)S(1)} %copy-done.3, f32[128,4096]{1,0:T(8,128)S(1)} %copy-done, f32[128,1024]{1,0:T(8,128)S(1)} %copy-done.1, f32[128,1024]{1,0:T(8,128)S(1)} %copy-done.2), custom_call_target="tpu_custom_call" | custom-call | tf_op jit(solution)/shard_map/pallas_call | solution.py:600
Async XLA Ops:
  128.9 1.6 %copy-start = (f32[128,4096]{1,0:T(8,128)S(1)}, f32[128,4096]{1,0:T(8,128)}, u32[]{:S(2)}) copy-start(f32[128,4096]{1,0:T(8,128)} %get-tuple-element.9.refs_1_) | copy-start | bytes 6291460
  130.5 1.0 copy-start.1
  131.6 1.0 copy-start.2
  132.6 0.9 copy-start.3
